TPU v7x, 128 devices: a whole 4x4x4 slice. The times are simulated.
128 devices in a mesh: sp: 32 (over z, y, core), tp: 4 (over x).
Axes of the slice: x: 4, y: 4, z: 4, core: 2. Of those that a mesh axis runs over, the one named last changes fastest.
Arguments:
- residual_in: bfloat16 [65536, 2048], P(('sp', 'tp')), may hold values from -6 to 6
- conv_input: bfloat16 [65536, 1024], P('sp', 'tp'), may hold values from -6 to 6
- input_gate: bfloat16 [65536, 1024], P('sp', 'tp'), may hold values from -6 to 6
- output_gate: bfloat16 [65536, 1024], P('sp', 'tp'), may hold values from -6 to 6
- conv_taps: bfloat16 [3, 1024], P(None, 'tp'), may hold values from -3.5 to 3.5
- doc_ids: int32 [65536], P('sp'), may hold values from 0 to 15, never falling along the last dimension, each value on 1 to 8192 neighbouring positions
- proj_weight: bfloat16 [1024, 2048], replicated, may hold values from -0.1875 to 0.1875
- norm_gain: float32 [2048], replicated, may hold values from 0.1 to 1.9
- expert_ids: int32 [65536, 2], P(('sp', 'tp')), may hold values from 0 to 31, all different within a row; in each aligned block of 512 rows (0 to 511, 512 to 1023, ...) at most 64 rows name the same one
- expert_weight: float32 [65536, 2], P(('sp', 'tp')), may hold values from 0.05 to 1
- w_gate: bfloat16 [32, 2048, 512], P('sp'), may hold values from -0.125 to 0.125
- w_up: bfloat16 [32, 2048, 512], P('sp'), may hold values from -0.125 to 0.125
- w_down: bfloat16 [32, 512, 2048], P('sp'), may hold values from -0.25 to 0.25
Outputs:
- layer_out: bfloat16 [65536, 2048], P(('sp', 'tp'))
Inputs may be any that keep to these rules, and one draw needn't show every extreme that they name: `doc_ids`: numbers never fall along the sequence; one document spans at most 8192 positions. `expert_ids`: a token's two experts differ; in each aligned block of rows that one device holds, no expert is named more than 64 times, a bound that some block reaches.
All inputs are finite; a program needn't handle non-finite values.
Results may differ from a plain program's by a relative error of at most 0.0047.
Values may be sent and summed in bfloat16 or wider, within the bound.
A program may use at most 128 MiB of HBM per device.

v0:
```python
import jax
import jax.numpy as jnp
from jax import lax
from jax.sharding import PartitionSpec as P

EXPERTS = 32
CAP = 64
epsilon = 1e-06
F32 = jnp.float32
BF16 = jnp.bfloat16


def from_behind(x, axis, by):
    devices = lax.axis_size(axis)
    pairs = [(i, i + by) for i in range(devices) if 0 <= i + by < devices]
    return lax.ppermute(x, axis, pairs)


def per_device(
    residual_in,
    conv_input,
    input_gate,
    output_gate,
    conv_taps,
    doc_ids,
    proj_weight,
    norm_gain,
    expert_ids,
    expert_weight,
    w_gate,
    w_up,
    w_down,
):
    kernel_width = conv_taps.shape[0]
    rim = kernel_width - 1
    length, channels = conv_input.shape
    doc_float = doc_ids.astype(F32)
    tail = input_gate[-rim:].astype(F32) * conv_input[-rim:].astype(F32)
    packed = jnp.concatenate([tail, jnp.broadcast_to(doc_float[-rim:, None], (rim, 128))], axis=1)
    prev = from_behind(packed, "sp", 1)
    prev_in, prev_ids = (prev[:, :channels], prev[:, channels])
    first = lax.axis_index("sp") == 0
    prev_ids = jnp.where(first, -1.0, prev_ids)
    product = input_gate.astype(F32) * conv_input.astype(F32)
    padded_in = jnp.concatenate([prev_in, product], axis=0)
    padded_ids = jnp.concatenate([prev_ids, doc_float], axis=0)
    conv_sum = jnp.zeros(product.shape, F32)
    for offset in range(kernel_width):
        same_doc = padded_ids[offset : offset + length] == doc_float
        term = conv_taps[offset].astype(F32)[None, :] * padded_in[offset : offset + length]
        conv_sum = conv_sum + jnp.where(same_doc[:, None], term, 0.0)
    gated = (output_gate.astype(F32) * conv_sum).astype(BF16)
    regrouped = lax.all_to_all(gated, "tp", split_axis=0, concat_axis=1, tiled=True)
    tokens = expert_ids.shape[0]
    experts = jnp.arange(EXPERTS, dtype=jnp.int32)
    ids_t = expert_ids.T
    weight_t = expert_weight.T
    hit = [ids_t[j][None, :] == experts[:, None] for j in range(2)]
    used = hit[0] | hit[1]
    weight_of = jnp.where(hit[0], weight_t[0][None, :], 0.0) + jnp.where(
        hit[1], weight_t[1][None, :], 0.0
    )
    t_row = lax.broadcasted_iota(jnp.int32, (tokens, tokens), 0)
    t_col = lax.broadcasted_iota(jnp.int32, (tokens, tokens), 1)
    earlier = (t_row < t_col).astype(BF16)
    rank = jnp.dot(used.astype(BF16), earlier, preferred_element_type=F32)
    code = jnp.where(used, rank, -1.0)
    slot_of = lax.broadcasted_iota(jnp.int32, (EXPERTS, CAP, tokens), 1).astype(F32)
    match = code[:, None, :] == slot_of
    dispatch = match.astype(BF16).reshape(EXPERTS * CAP, tokens)
    combine = (
        jnp.where(match, weight_of[:, None, :], 0.0).astype(BF16).reshape(EXPERTS * CAP, tokens)
    )
    mixed = jnp.dot(regrouped, proj_weight, preferred_element_type=F32)
    hidden = residual_in.astype(F32) + mixed
    scale_rows = lax.rsqrt(jnp.mean(hidden * hidden, axis=-1, keepdims=True) + epsilon)
    normed = (hidden * scale_rows * norm_gain[None, :]).astype(BF16)
    width = normed.shape[1]
    buffer = jnp.dot(dispatch, normed, preferred_element_type=F32).astype(BF16)
    buffer = buffer.reshape(EXPERTS, CAP, width)
    slots = lax.all_to_all(buffer, "sp", split_axis=0, concat_axis=0, tiled=True).reshape(
        EXPERTS * CAP, width
    )
    gate_val = jnp.dot(slots, w_gate[0], preferred_element_type=F32)
    up_val = jnp.dot(slots, w_up[0], preferred_element_type=F32)
    act_rows = (jax.nn.silu(gate_val) * up_val).astype(BF16)
    expert_out = jnp.dot(act_rows, w_down[0], preferred_element_type=F32).astype(BF16)
    expert_out = expert_out.reshape(EXPERTS, CAP, width)
    returned = lax.all_to_all(expert_out, "sp", split_axis=0, concat_axis=0, tiled=True).reshape(
        EXPERTS * CAP, width
    )
    expert_sum = lax.dot_general(
        combine, returned, (((0,), (0,)), ((), ())), preferred_element_type=F32
    )
    return (hidden + expert_sum).astype(BF16)


def solution(mesh):
    return jax.shard_map(
        per_device,
        mesh=mesh,
        in_specs=(
            P(("sp", "tp"), None),
            P("sp", "tp"),
            P("sp", "tp"),
            P("sp", "tp"),
            P(None, "tp"),
            P("sp"),
            P(),
            P(),
            P(("sp", "tp"), None),
            P(("sp", "tp"), None),
            P("sp", None, None),
            P("sp", None, None),
            P("sp", None, None),
        ),
        out_specs=P(("sp", "tp"), None),
        check_vma=False,
    )
```

profile of v0, /device:TPU:0, one launch (start us, length us, event | category | flops | bytes accessed | tf_op | source)
XLA Modules:
  0.0 288.9 jit_solution(236948942608263788)
XLA Ops:
  0.0 0.0 copy-start
  0.0 0.8 convert_element_type.61
  0.9 0.1 slice.64
  0.9 0.7 convert_multiply_fusion.1
  1.6 0.1 broadcast_in_dim.85
  1.7 1.4 collective-permute-start
  3.2 3.1 %convert_multiply_fusion = f32[2048,256]{1,0:T(8,128)} fusion(bf16[2048,256]{1,0:T(8,128)(2,1)} %param.14, bf16[2048,256]{1,0:T(8,128)(2,1)} %param.15), kind=kLoop, calls=%fused_computation.31 | loop fusion | flops 1572864 | bytes 4194304 | tf_op jit(solution)/shard_map/mul | solution.py:44
  6.2 0.0 copy-done.5
  6.3 0.0 copy-done.6
  6.3 0.0 collective-permute-done
  6.3 0.1 fusion.27
  6.4 0.1 fusion.25
  6.5 5.9 %fusion.7 = bf16[2048,256]{1,0:T(8,128)(2,1)} fusion(f32[2,256]{1,0:T(2,128)S(1)} %slice.68, f32[2048,256]{1,0:T(8,128)} %convert_multiply_fusion, bf16[2048,256]{1,0:T(8,128)(2,1)S(1)} %copy-done.4, f32[256]{0:T(256)S(1)} %bitcast.51, f32[256]{0:T(256)S(1)} %bitcast.52, f32[256]{0:T(256)S(1)} %bitcast.50, pred[2048]{0:T(1024)(128)(4,1)S(1)} %convert_compare_fusion, ...), kind=kLoop, calls=%fused_computation.18 | loop fusion | flops 6815744 | bytes 4205568 | tf_op jit(solution)/shard_map/convert_element_type | solution.py:52
  12.4 5.0 %all-to-all-start = ((bf16[4,512,256]{2,1,0:T(8,128)(2,1)}), bf16[4,512,256]{2,1,0:T(8,128)(2,1)S(1)}, u32[]{:S(2)}, u32[]{:S(2)}) async-start(bf16[4,512,256]{2,1,0:T(8,128)(2,1)} %bitcast.43), calls=%async_computation | async-start | bytes 2097152 | tf_op jit(solution)/shard_map/all_to_all | solution.py:53
  17.4 0.1 iota.41
  17.5 0.2 convolution_select_fusion
  17.7 1.6 bitcast_compare_fusion
  19.3 14.0 %all-to-all-done = bf16[4,512,256]{2,1,0:T(8,128)(2,1)S(1)} async-done(((bf16[4,512,256]{2,1,0:T(8,128)(2,1)}), bf16[4,512,256]{2,1,0:T(8,128)(2,1)S(1)}, u32[]{:S(2)}, u32[]{:S(2)}) %all-to-all-start) | async-done | bytes 1048608 | tf_op jit(solution)/shard_map/all_to_all | solution.py:53
  33.3 1.0 copy-done.2
  34.3 1.5 copy.15
  35.8 0.0 copy-start.3
  35.8 0.0 copy-start.11
  35.8 5.8 %multiply_reduce_fusion = (f32[512]{0:T(512)S(1)}, f32[512,2048]{1,0:T(8,128)S(1)}) fusion(bf16[512,1024]{0,1:T(8,128)(2,1)S(1)} %bitcast.41, bf16[1024,2048]{1,0:T(8,128)(2,1)} %param.19, bf16[512,2048]{1,0:T(8,128)(2,1)} %param.13), kind=kOutput, calls=%fused_computation.7 | convolution fusion | flops 2151677440 | bytes 11536384 | tf_op jit(solution)/shard_map/dot_general | solution.py:74
  41.6 5.1 %convolution_convert_fusion.1 = bf16[2048,2048]{1,0:T(8,128)(2,1)S(1)} fusion(pred[2048,512]{1,0:T(32,128)(4,1)S(1)} %copy-done.3, f32[512,2048]{1,0:T(8,128)S(1)} %get-tuple-element.15, f32[2048]{0:T(1024)S(1)} %copy-done.11, f32[512]{0:T(512)S(1)} %add_rsqrt_fusion), kind=kOutput, calls=%fused_computation.1 | convolution fusion | flops 4302307328 | bytes 13641728 | tf_op jit(solution)/shard_map/dot_general | solution.py:79
  46.7 0.0 copy-start.9
  46.7 104.8 %all_to_all.29 = bf16[32,64,2048]{2,1,0:T(8,128)(2,1)S(1)} all-to-all(bf16[32,64,2048]{2,1,0:T(8,128)(2,1)S(1)} %bitcast.38), channel_id=1, replica_groups=mesh['sp'=32,'tp'=4] {'sp'}, dimensions={0} | all-to-all | bytes 16777216 | tf_op jit(solution)/shard_map/all_to_all | solution.py:81
  151.5 4.5 %fusion.12 = f32[2048,512]{1,0:T(8,128)S(1)} fusion(bf16[2048,2048]{1,0:T(8,128)(2,1)S(1)} %bitcast.39, bf16[1,2048,512]{2,1,0:T(8,128)(2,1)S(1)} %copy-done.9), kind=kOutput, calls=%fused_computation.24 | convolution fusion | flops 4294967296 | bytes 14680064 | tf_op jit(solution)/shard_map/dot_general | solution.py:84
  156.1 5.2 %multiply_convert_fusion = bf16[2048,512]{1,0:T(8,128)(2,1)S(1)} fusion(f32[2048,512]{1,0:T(8,128)S(1)} %fusion.12, bf16[2048,2048]{1,0:T(8,128)(2,1)S(1)} %bitcast.40, bf16[1,2048,512]{2,1,0:T(8,128)(2,1)S(1)} %copy-done.10), kind=kOutput, calls=%fused_computation.5 | convolution fusion | flops 4301258752 | bytes 16777216 | tf_op jit(solution)/shard_map/dot_general | solution.py:85
  161.2 6.7 %convolution_convert_fusion = bf16[2048,2048]{1,0:T(8,128)(2,1)} fusion(bf16[2048,512]{1,0:T(8,128)(2,1)S(1)} %multiply_convert_fusion, bf16[1,512,2048]{2,1,0:T(8,128)(2,1)S(1)} %copy-done), kind=kOutput, calls=%fused_computation | convolution fusion | flops 4299161600 | bytes 12582912 | tf_op jit(solution)/shard_map/dot_general | solution.py:87
  168.0 5.1 %all-to-all-start.2 = ((bf16[32,64,2048]{2,1,0:T(8,128)(2,1)}), bf16[32,64,2048]{2,1,0:T(8,128)(2,1)}, u32[]{:S(2)}, u32[]{:S(2)}) async-start(bf16[32,64,2048]{2,1,0:T(8,128)(2,1)} %bitcast.37), calls=%async_computation.2 | async-start | bytes 16777216 | tf_op jit(solution)/shard_map/all_to_all | solution.py:89
  173.1 105.8 %all-to-all-done.2 = bf16[32,64,2048]{2,1,0:T(8,128)(2,1)} async-done(((bf16[32,64,2048]{2,1,0:T(8,128)(2,1)}), bf16[32,64,2048]{2,1,0:T(8,128)(2,1)}, u32[]{:S(2)}, u32[]{:S(2)}) %all-to-all-start.2) | async-done | bytes 8388640 | tf_op jit(solution)/shard_map/all_to_all | solution.py:89
  279.0 9.9 %fusion = bf16[512,2048]{1,0:T(8,128)(2,1)} fusion(f32[512,2048]{1,0:T(8,128)} %copy-done.1, bf16[32,64,2048]{2,1,0:T(8,128)(2,1)} %all-to-all-done.2, bf16[32,512]{1,0:T(8,128)(2,1)S(1)} %select_add_fusion, f32[32,512]{1,0:T(8,128)S(1)} %convolution_select_fusion, f32[64]{0:T(128)S(1)} %iota_convert_fusion), kind=kOutput, calls=%fused_computation.3 | convolution fusion | flops 4299161600 | bytes 14778624 | tf_op jit(solution)/shard_map/dot_general | solution.py:92
  (27 shorter events, 0.1 us)
Async XLA Ops:
  0.0 161.2 %copy-start = (bf16[1,512,2048]{2,1,0:T(8,128)(2,1)S(1)}, bf16[1,512,2048]{2,1,0:T(8,128)(2,1)}, u32[]{:S(2)}) copy-start(bf16[1,512,2048]{2,1,0:T(8,128)(2,1)} %param.25) | copy-start | bytes 6291460
  0.9 5.4 %copy-start.5 = (s32[2048]{0:T(1024)S(1)}, s32[2048]{0:T(1024)}, u32[]{:S(2)}) copy-start(s32[2048]{0:T(1024)} %param.18) | copy-start | bytes 24580
  1.7 4.5 %copy-start.6 = (bf16[3,256]{1,0:T(4,128)(2,1)S(1)}, bf16[3,256]{1,0:T(4,128)(2,1)}, u32[]{:S(2)}) copy-start(bf16[3,256]{1,0:T(4,128)(2,1)} %param.17) | copy-start | bytes 4612
  1.7 4.8 %copy-start.4 = (bf16[2048,256]{1,0:T(8,128)(2,1)S(1)}, bf16[2048,256]{1,0:T(8,128)(2,1)}, u32[]{:S(2)}) copy-start(bf16[2048,256]{1,0:T(8,128)(2,1)} %param.16) | copy-start | bytes 3145732
  1.7 4.6 %collective-permute-start = (f32[2,384]{1,0:T(2,128)S(1)}, f32[2,384]{1,0:T(2,128)S(1)}, u32[]{:S(2)}, u32[]{:S(2)}) collective-permute-start(f32[2,384]{1,0:T(2,128)S(1)} %pad_maximum_fusion.2), channel_id=1, source_target_pairs={{0,4},{4,8},{8,12},{12,16},{16,20},{20,24},{24,28},{28,32},{32,36}... | collective-permute-start | bytes 9224 | tf_op jit(solution)/shard_map/ppermute | solution.py:16
  12.4 5.1 %copy-start.7 = (s32[512,2]{0,1:T(2,128)S(1)}, s32[512,2]{0,1:T(2,128)}, u32[]{:S(2)}) copy-start(s32[512,2]{0,1:T(2,128)} %param.21) | copy-start | bytes 12292
  12.4 20.9 %all-to-all-start = ((bf16[4,512,256]{2,1,0:T(8,128)(2,1)}), bf16[4,512,256]{2,1,0:T(8,128)(2,1)S(1)}, u32[]{:S(2)}, u32[]{:S(2)}) async-start(bf16[4,512,256]{2,1,0:T(8,128)(2,1)} %bitcast.43), calls=%async_computation | async-start | bytes 2097152 | tf_op jit(solution)/shard_map/all_to_all | solution.py:53
  33.3 1.0 copy-start.2
  35.8 5.8 %copy-start.3 = (pred[2048,512]{1,0:T(32,128)(4,1)S(1)}, pred[2048,512]{1,0:T(32,128)(4,1)}, u32[]{:S(2)}) copy-start(pred[2048,512]{1,0:T(32,128)(4,1)} %bitcast_compare_fusion) | copy-start | bytes 3145732
  35.8 5.8 %copy-start.11 = (f32[2048]{0:T(1024)S(1)}, f32[2048]{0:T(1024)}, u32[]{:S(2)}) copy-start(f32[2048]{0:T(1024)} %param.20) | copy-start | bytes 24580
  41.6 5.1 %copy-start.1 = (f32[512,2048]{1,0:T(8,128)}, f32[512,2048]{1,0:T(8,128)S(1)}, u32[]{:S(2)}) copy-start(f32[512,2048]{1,0:T(8,128)S(1)} %get-tuple-element.15) | copy-start | bytes 12582916
  46.7 104.8 %copy-start.9 = (bf16[1,2048,512]{2,1,0:T(8,128)(2,1)S(1)}, bf16[1,2048,512]{2,1,0:T(8,128)(2,1)}, u32[]{:S(2)}) copy-start(bf16[1,2048,512]{2,1,0:T(8,128)(2,1)} %param.23) | copy-start | bytes 6291460
  151.5 4.5 %copy-start.10 = (bf16[1,2048,512]{2,1,0:T(8,128)(2,1)S(1)}, bf16[1,2048,512]{2,1,0:T(8,128)(2,1)}, u32[]{:S(2)}) copy-start(bf16[1,2048,512]{2,1,0:T(8,128)(2,1)} %param.24) | copy-start | bytes 6291460
  168.0 5.1 %copy-start.8 = (f32[512,2]{0,1:T(2,128)S(1)}, f32[512,2]{0,1:T(2,128)}, u32[]{:S(2)}) copy-start(f32[512,2]{0,1:T(2,128)} %param.22) | copy-start | bytes 12292
  168.0 111.0 %all-to-all-start.2 = ((bf16[32,64,2048]{2,1,0:T(8,128)(2,1)}), bf16[32,64,2048]{2,1,0:T(8,128)(2,1)}, u32[]{:S(2)}, u32[]{:S(2)}) async-start(bf16[32,64,2048]{2,1,0:T(8,128)(2,1)} %bitcast.37), calls=%async_computation.2 | async-start | bytes 16777216 | tf_op jit(solution)/shard_map/all_to_all | solution.py:89
where the time goes:
time: 289 us
  waiting for transfers between devices  120 us (42%)
  blocking collectives  105 us (36%)
  matrix products  37.4 us (13%)
  other arithmetic  12.4 us (4%)
  starting transfers between devices  11.5 us (4%)
    all_to_all x1, waiting for transfers between devices, per_device(): lax.all_to_all(expert_out, 'sp', split_axis=0, concat_axis=0, tiled=True)  106 us
    all_to_all x1, blocking collectives, per_device(): lax.all_to_all(buffer, 'sp', split_axis=0, concat_axis=0, tiled=True)  105 us
    all_to_all x1, waiting for transfers between devices, per_device(): lax.all_to_all(gated, 'tp', split_axis=0, concat_axis=1, tiled=True)  14 us
    dot_general x1, matrix products, per_device(): lax.dot_general(combine, returned, (((0,), (0,)), ((), ())), preferred_el...  9.88 us
    dot_general x1, matrix products, per_device(): jnp.dot(act_rows, w_down[0], preferred_element_type=F32).astype(BF16)  6.74 us
    convert_element_type x1, other arithmetic, per_device(): gated = (output_gate.astype(F32) * conv_sum).astype(BF16)  5.9 us
    dot_general x1, matrix products, per_device(): mixed = jnp.dot(regrouped, proj_weight, preferred_element_type=F32)  5.8 us
  transfers between devices with their start and end apart: 3, of which 2 were waited for; matrix products, arithmetic and copies ran while one was open for 2% of the time, Pallas kernels for 0%

commit v1 on v0

--- a/solution.py
+++ b/solution.py
@@ -50,7 +50,13 @@
         term = conv_taps[offset].astype(F32)[None, :] * padded_in[offset : offset + length]
         conv_sum = conv_sum + jnp.where(same_doc[:, None], term, 0.0)
     gated = (output_gate.astype(F32) * conv_sum).astype(BF16)
-    regrouped = lax.all_to_all(gated, "tp", split_axis=0, concat_axis=1, tiled=True)
+    f_next = lax.all_to_all(
+        jnp.stack(jnp.split(gated, lax.axis_size("tp"), axis=0)),
+        axis_name="tp",
+        split_axis=0,
+        concat_axis=0,
+    )
+    regrouped = jnp.concatenate(f_next, axis=1)
     tokens = expert_ids.shape[0]
     experts = jnp.arange(EXPERTS, dtype=jnp.int32)
     ids_t = expert_ids.T

time: 289 us -> 292 us (1.010)
  local copies, waits for them, and re-layouts: 2.74 us -> 5.74 us
    unnamed x24 -> x25, local copies, waits for them, and re-layouts: 1.02 us -> 5.29 us
  transfers between devices with their start and end apart: 3 -> 3, of which waited for: 2 -> 2; matrix products, arithmetic and copies ran while one was open for 2% -> 4% of each run, Pallas kernels for 0% -> 0%
where the time goes in v1:
time: 292 us
  waiting for transfers between devices  120 us (41%)
  blocking collectives  105 us (36%)
  matrix products  37.3 us (13%)
  other arithmetic  12.9 us (4%)
  starting transfers between devices  11.2 us (4%)
  local copies, waits for them, and re-layouts  5.74 us (2%)
    all_to_all x1, waiting for transfers between devices, per_device(): lax.all_to_all(expert_out, 'sp', split_axis=0, concat_axis=0, tiled=True)  106 us
    all_to_all x1, blocking collectives, per_device(): lax.all_to_all(buffer, 'sp', split_axis=0, concat_axis=0, tiled=True)  105 us
    all_to_all x1, waiting for transfers between devices, per_device(): lax.all_to_all(jnp.stack(jnp.split(gated, lax.axis_size('tp'), axis=0)),...  14 us
    dot_general x1, matrix products, per_device(): lax.dot_general(combine, returned, (((0,), (0,)), ((), ())), preferred_el...  9.88 us
    dot_general x1, matrix products, per_device(): jnp.dot(act_rows, w_down[0], preferred_element_type=F32).astype(BF16)  6.71 us
  transfers between devices with their start and end apart: 3, of which 2 were waited for; matrix products, arithmetic and copies ran while one was open for 4% of the time, Pallas kernels for 0%

profile of v1, /device:TPU:0, one launch (start us, length us, event | category | flops | bytes accessed | tf_op | source)
XLA Modules:
  0.0 292.0 jit_solution(3263590335518976606)
XLA Ops:
  0.0 0.9 convert_element_type.61
  0.9 0.1 slice.64
  0.9 0.7 convert_multiply_fusion.1
  1.7 0.1 broadcast_in_dim.85
  1.7 0.1 copy.19
  1.9 1.3 collective-permute-start
  3.2 1.5 copy.20
  4.7 2.3 copy.21
  7.0 0.6 convert_compare_fusion
  7.5 2.9 convert_multiply_fusion
  10.4 0.6 slice_convert_fusion.2
  11.0 1.5 copy.18
  12.6 0.1 fusion.25
  12.7 4.4 %fusion.7 = bf16[2048,256]{0,1:T(8,128)(2,1)S(1)} fusion(f32[2,256]{0,1:T(8,128)S(1)} %slice.68, f32[2048,256]{0,1:T(8,128)} %convert_multiply_fusion, bf16[2048,256]{0,1:T(8,128)(2,1)S(1)} %copy.18, f32[256]{0:T(256)} %bitcast.59, f32[256]{0:T(256)} %bitcast.60, f32[256]{0:T(256)} %bitcast.58, pred[2048]{0:T(1024)(128)(4,1)S(1)} %copy-done.4, ...), kind=kLoop, calls=%fused_computation.18 | loop fusion | flops 6815744 | bytes 4205568 | tf_op jit(solution)/shard_map/convert_element_type | solution.py:52
  17.0 0.1 slice_bitcast_fusion.3
  17.1 0.0 copy-start.6
  17.1 1.1 pad_maximum_fusion.1
  18.2 4.9 %all-to-all-start = ((bf16[4,512,256]{1,2,0:T(8,128)(2,1)}), bf16[4,512,256]{1,2,0:T(8,128)(2,1)S(1)}, u32[]{:S(2)}, u32[]{:S(2)}) async-start(bf16[4,512,256]{1,2,0:T(8,128)(2,1)} %pad_maximum_fusion.1), calls=%async_computation | async-start | bytes 2097152 | tf_op jit(solution)/shard_map/all_to_all | solution.py:53
  23.1 0.1 iota.41
  23.2 0.2 convolution_select_fusion
  23.4 1.6 bitcast_compare_fusion
  25.0 14.0 %all-to-all-done = bf16[4,512,256]{1,2,0:T(8,128)(2,1)S(1)} async-done(((bf16[4,512,256]{1,2,0:T(8,128)(2,1)}), bf16[4,512,256]{1,2,0:T(8,128)(2,1)S(1)}, u32[]{:S(2)}, u32[]{:S(2)}) %all-to-all-start) | async-done | bytes 1048608 | tf_op jit(solution)/shard_map/all_to_all | solution.py:53
  39.0 5.8 %multiply_reduce_fusion = (f32[512]{0:T(512)S(1)}, f32[512,2048]{1,0:T(8,128)S(1)}) fusion(bf16[512,1024]{0,1:T(8,128)(2,1)S(1)} %bitcast.51, bf16[1024,2048]{1,0:T(8,128)(2,1)} %param.19, bf16[512,2048]{1,0:T(8,128)(2,1)} %param.13), kind=kOutput, calls=%fused_computation.7 | convolution fusion | flops 2151677440 | bytes 11536384 | tf_op jit(solution)/shard_map/dot_general | solution.py:80
  44.8 5.1 %convolution_convert_fusion.1 = bf16[2048,2048]{1,0:T(8,128)(2,1)S(1)} fusion(pred[2048,512]{1,0:T(32,128)(4,1)S(1)} %copy-done.2, f32[512,2048]{1,0:T(8,128)S(1)} %get-tuple-element.19, f32[2048]{0:T(1024)S(1)} %copy-done.10, f32[512]{0:T(512)S(1)} %add_rsqrt_fusion), kind=kOutput, calls=%fused_computation.1 | convolution fusion | flops 4302307328 | bytes 13641728 | tf_op jit(solution)/shard_map/dot_general | solution.py:85
  49.9 0.0 copy-start.8
  50.0 104.8 %all_to_all.15 = bf16[32,64,2048]{2,1,0:T(8,128)(2,1)S(1)} all-to-all(bf16[32,64,2048]{2,1,0:T(8,128)(2,1)S(1)} %bitcast.48), channel_id=1, replica_groups=mesh['sp'=32,'tp'=4] {'sp'}, dimensions={0} | all-to-all | bytes 16777216 | tf_op jit(solution)/shard_map/all_to_all | solution.py:87
  154.7 4.5 %fusion.12 = f32[2048,512]{1,0:T(8,128)S(1)} fusion(bf16[2048,2048]{1,0:T(8,128)(2,1)S(1)} %bitcast.49, bf16[1,2048,512]{2,1,0:T(8,128)(2,1)S(1)} %copy-done.8), kind=kOutput, calls=%fused_computation.24 | convolution fusion | flops 4294967296 | bytes 14680064 | tf_op jit(solution)/shard_map/dot_general | solution.py:90
  159.3 5.2 %multiply_convert_fusion = bf16[2048,512]{1,0:T(8,128)(2,1)S(1)} fusion(f32[2048,512]{1,0:T(8,128)S(1)} %fusion.12, bf16[2048,2048]{1,0:T(8,128)(2,1)S(1)} %bitcast.50, bf16[1,2048,512]{2,1,0:T(8,128)(2,1)S(1)} %copy-done.9), kind=kOutput, calls=%fused_computation.5 | convolution fusion | flops 4301258752 | bytes 16777216 | tf_op jit(solution)/shard_map/dot_general | solution.py:91
  164.5 6.7 %convolution_convert_fusion = bf16[2048,2048]{1,0:T(8,128)(2,1)} fusion(bf16[2048,512]{1,0:T(8,128)(2,1)S(1)} %multiply_convert_fusion, bf16[1,512,2048]{2,1,0:T(8,128)(2,1)S(1)} %copy-done), kind=kOutput, calls=%fused_computation | convolution fusion | flops 4299161600 | bytes 12582912 | tf_op jit(solution)/shard_map/dot_general | solution.py:93
  171.2 5.1 %all-to-all-start.2 = ((bf16[32,64,2048]{2,1,0:T(8,128)(2,1)}), bf16[32,64,2048]{2,1,0:T(8,128)(2,1)}, u32[]{:S(2)}, u32[]{:S(2)}) async-start(bf16[32,64,2048]{2,1,0:T(8,128)(2,1)} %bitcast.47), calls=%async_computation.2 | async-start | bytes 16777216 | tf_op jit(solution)/shard_map/all_to_all | solution.py:95
  176.3 105.8 %all-to-all-done.2 = bf16[32,64,2048]{2,1,0:T(8,128)(2,1)} async-done(((bf16[32,64,2048]{2,1,0:T(8,128)(2,1)}), bf16[32,64,2048]{2,1,0:T(8,128)(2,1)}, u32[]{:S(2)}, u32[]{:S(2)}) %all-to-all-start.2) | async-done | bytes 8388640 | tf_op jit(solution)/shard_map/all_to_all | solution.py:95
  282.1 9.9 %fusion = bf16[512,2048]{1,0:T(8,128)(2,1)} fusion(f32[512,2048]{1,0:T(8,128)} %copy-done.1, bf16[32,64,2048]{2,1,0:T(8,128)(2,1)} %all-to-all-done.2, bf16[32,512]{1,0:T(8,128)(2,1)S(1)} %select_add_fusion, f32[32,512]{1,0:T(8,128)S(1)} %convolution_select_fusion, f32[64]{0:T(128)S(1)} %iota_convert_fusion), kind=kOutput, calls=%fused_computation.3 | convolution fusion | flops 4299161600 | bytes 14778624 | tf_op jit(solution)/shard_map/dot_general | solution.py:98
  (30 shorter events, 0.1 us)
Async XLA Ops:
  0.0 164.5 %copy-start = (bf16[1,512,2048]{2,1,0:T(8,128)(2,1)S(1)}, bf16[1,512,2048]{2,1,0:T(8,128)(2,1)}, u32[]{:S(2)}) copy-start(bf16[1,512,2048]{2,1,0:T(8,128)(2,1)} %param.25) | copy-start | bytes 6291460
  0.0 7.0 %copy-start.3 = (s32[2048]{0:T(1024)S(1)}, s32[2048]{0:T(1024)}, u32[]{:S(2)}) copy-start(s32[2048]{0:T(1024)} %param.18) | copy-start | bytes 24580
  1.9 10.7 %collective-permute-start = (f32[2,384]{0,1:T(8,128)S(1)}, f32[2,384]{0,1:T(8,128)S(1)}, u32[]{:S(2)}, u32[]{:S(2)}) collective-permute-start(f32[2,384]{0,1:T(8,128)S(1)} %copy.19), channel_id=1, source_target_pairs={{0,4},{4,8},{8,12},{12,16},{16,20},{20,24},{24,28},{28,32},{32,36}... | collective-permute-start | bytes 9224 | tf_op jit(solution)/shard_map/ppermute | solution.py:16
  7.0 3.5 %copy-start.5 = (bf16[3,256]{1,0:T(4,128)(2,1)S(1)}, bf16[3,256]{1,0:T(4,128)(2,1)}, u32[]{:S(2)}) copy-start(bf16[3,256]{1,0:T(4,128)(2,1)} %param.17) | copy-start | bytes 4612
  10.4 2.2 copy-start.4
  17.1 6.1 %copy-start.6 = (s32[512,2]{0,1:T(2,128)S(1)}, s32[512,2]{0,1:T(2,128)}, u32[]{:S(2)}) copy-start(s32[512,2]{0,1:T(2,128)} %param.21) | copy-start | bytes 12292
  18.2 20.8 %all-to-all-start = ((bf16[4,512,256]{1,2,0:T(8,128)(2,1)}), bf16[4,512,256]{1,2,0:T(8,128)(2,1)S(1)}, u32[]{:S(2)}, u32[]{:S(2)}) async-start(bf16[4,512,256]{1,2,0:T(8,128)(2,1)} %pad_maximum_fusion.1), calls=%async_computation | async-start | bytes 2097152 | tf_op jit(solution)/shard_map/all_to_all | solution.py:53
  39.0 5.8 %copy-start.2 = (pred[2048,512]{1,0:T(32,128)(4,1)S(1)}, pred[2048,512]{1,0:T(32,128)(4,1)}, u32[]{:S(2)}) copy-start(pred[2048,512]{1,0:T(32,128)(4,1)} %bitcast_compare_fusion) | copy-start | bytes 3145732
  39.0 5.8 %copy-start.10 = (f32[2048]{0:T(1024)S(1)}, f32[2048]{0:T(1024)}, u32[]{:S(2)}) copy-start(f32[2048]{0:T(1024)} %param.20) | copy-start | bytes 24580
  44.8 5.1 %copy-start.1 = (f32[512,2048]{1,0:T(8,128)}, f32[512,2048]{1,0:T(8,128)S(1)}, u32[]{:S(2)}) copy-start(f32[512,2048]{1,0:T(8,128)S(1)} %get-tuple-element.19) | copy-start | bytes 12582916
  49.9 104.8 %copy-start.8 = (bf16[1,2048,512]{2,1,0:T(8,128)(2,1)S(1)}, bf16[1,2048,512]{2,1,0:T(8,128)(2,1)}, u32[]{:S(2)}) copy-start(bf16[1,2048,512]{2,1,0:T(8,128)(2,1)} %param.23) | copy-start | bytes 6291460
  154.7 4.5 %copy-start.9 = (bf16[1,2048,512]{2,1,0:T(8,128)(2,1)S(1)}, bf16[1,2048,512]{2,1,0:T(8,128)(2,1)}, u32[]{:S(2)}) copy-start(bf16[1,2048,512]{2,1,0:T(8,128)(2,1)} %param.24) | copy-start | bytes 6291460
  171.2 5.1 %copy-start.7 = (f32[512,2]{0,1:T(2,128)S(1)}, f32[512,2]{0,1:T(2,128)}, u32[]{:S(2)}) copy-start(f32[512,2]{0,1:T(2,128)} %param.22) | copy-start | bytes 12292
  171.2 111.0 %all-to-all-start.2 = ((bf16[32,64,2048]{2,1,0:T(8,128)(2,1)}), bf16[32,64,2048]{2,1,0:T(8,128)(2,1)}, u32[]{:S(2)}, u32[]{:S(2)}) async-start(bf16[32,64,2048]{2,1,0:T(8,128)(2,1)} %bitcast.47), calls=%async_computation.2 | async-start | bytes 16777216 | tf_op jit(solution)/shard_map/all_to_all | solution.py:95
